TPU v7x, 128 devices: a whole 4x4x4 slice. The times are simulated.
128 devices in a mesh: rep: 2 (over z_hi), fs: 32 (over z_lo, y, x), tp: 2 (over core).
Axes of the slice: x: 4, y: 4, z: 4 (z_hi: 2, z_lo: 2; z = z_hi * 2 + z_lo), core: 2. Of those that a mesh axis runs over, the one named last changes fastest.
Arguments:
- resid: bfloat16 [65536, 2048], P(('rep', 'fs'), 'tp'), may hold values from -6 to 6
- gain_mix_in: float32 [2048], replicated, may hold values from 0.1 to 1.9
- u_weight: float32 [2048, 1024], P('fs', 'tp'), may hold values from -0.125 to 0.125
- v_weight: float32 [2048, 1024], P('fs', 'tp'), may hold values from -0.125 to 0.125
- u_scale: float32 [1024], P('tp'), may hold values from 0.5 to 2
- v_scale: float32 [1024], P('tp'), may hold values from 0.3 to 3
- v_gain: float32 [1024], P('tp'), may hold values from 0.1 to 1.9
- mix_matrix: float32 [16, 128, 128], P('tp'), may hold values from -0.5 to 0.5
- mix_bias: float32 [16, 128], P('tp'), may hold values from 0.1 to 1.9
- out_weight: float32 [1024, 2048], P('tp', 'fs'), may hold values from -0.1875 to 0.1875
- out_scale: float32 [2048], P('fs'), may hold values from 0.3 to 3
- gain_mix_out: float32 [2048], replicated, may hold values from 0.1 to 1.9
- gain_ffn_in: float32 [2048], replicated, may hold values from 0.1 to 1.9
- up_weight: float32 [2048, 4096], P('fs', 'tp'), may hold values from -0.125 to 0.125
- up_scale: float32 [4096], P('tp'), may hold values from 0.5 to 2
- down_weight: float32 [4096, 2048], P('tp', 'fs'), may hold values from -0.09375 to 0.09375
- down_scale: float32 [2048], P('fs'), may hold values from 0.3 to 3
- gain_ffn_out: float32 [2048], replicated, may hold values from 0.1 to 1.9
Outputs:
- result: bfloat16 [65536, 2048], P(('rep', 'fs'), 'tp')
All inputs are finite; a program needn't handle non-finite values.
Results may differ from a plain program's by a relative error of at most 0.013.
Values may be sent and summed in bfloat16 or wider, within the bound.
No kernel may reach another device: no remote copies, remote signals or barrier semaphores. Data moves between devices by JAX's collectives and lax.ppermute only.
A program may use at most 128 MiB of HBM per device.

v0:
```python
import jax
import jax.numpy as jnp
from jax import lax
from jax.sharding import PartitionSpec as P


def turned_gather(arrays, axis, dims):
    turned = [jnp.moveaxis(a, dim, 0) for a, dim in zip(arrays, dims)]
    widths = [t[0].size for t in turned]
    both = jnp.concatenate([t.reshape(-1, w) for t, w in zip(turned, widths)], axis=1)
    result = lax.all_gather(both, axis, axis=0, tiled=True)
    pieces = jnp.split(result, [sum(widths[:k]) for k in range(1, len(widths))], axis=1)
    return tuple(
        (
            jnp.moveaxis(b.reshape(-1, *t.shape[1:]), 0, dim)
            for b, t, dim in zip(pieces, turned, dims)
        )
    )


def in_one_piece(arrays, axis, dim, along):
    ends, at = ([], 0)
    for a in arrays[:-1]:
        at += a.shape[along]
        ends.append(at)
    both = jnp.concatenate(arrays, axis=along)
    return tuple(jnp.split(lax.all_gather(both, axis, axis=dim, tiled=True), ends, axis=along))


def copy_for_each(array, axis):
    copies = jnp.broadcast_to(array, (lax.axis_size(axis), *array.shape))
    return lax.all_to_all(copies, axis, split_axis=0, concat_axis=0, tiled=True)


def over_copies(array, axis):
    return copy_for_each(array, axis).sum(axis=0)


def packed_total(arrays, axis):
    vector, at, gathered = (jnp.concatenate([a.reshape(-1) for a in arrays]), 0, [])
    running = over_copies(vector, axis)
    for a in arrays:
        gathered.append(running[at : at + a.size].reshape(a.shape))
        at += a.size
    return tuple(gathered)


def in_order(pieces, dim):
    dims = list(pieces.shape[1:])
    dims[dim] *= pieces.shape[0]
    return jnp.moveaxis(pieces, 0, dim).reshape(dims)


def gathered_copies(array, axis, dim):
    pieces = copy_for_each(array, axis)
    return in_order(pieces, dim)


def total_of_pieces(array, axis):
    pieces = lax.all_gather(array, axis).astype(jnp.float32)
    return pieces.sum(axis=0)


def in_blocks(array, dim, peers):
    before, after = (array.shape[:dim], array.shape[dim + 1 :])
    return jnp.moveaxis(array.reshape(*before, peers, -1, *after), dim, 0)


def sent_and_summed(array, axis, dim):
    peers = lax.axis_size(axis)
    pieces = lax.all_to_all(in_blocks(array, dim, peers), axis, 0, 0, tiled=True)
    return jnp.sum(pieces.astype(jnp.float32), axis=0)


def rms_norm(values, gain, width, power_sum):
    return values * lax.rsqrt(power_sum / width + 1e-06) * gain


def local(
    resid,
    gain_mix_in,
    u_weight,
    v_weight,
    u_scale,
    v_scale,
    v_gain,
    mix_matrix,
    mix_bias,
    out_weight,
    out_scale,
    gain_mix_out,
    gain_ffn_in,
    up_weight,
    up_scale,
    down_weight,
    down_scale,
    gain_ffn_out,
):
    rows = resid.shape[0]
    part_width = resid.shape[1]
    width = part_width * lax.axis_size("tp")
    lane = lax.axis_index("tp")
    full_rows = lax.all_gather(resid, "tp", axis=1, tiled=True)
    out_scales, down_scales = turned_gather((out_scale, down_scale), "fs", (0, 0))
    full_float = full_rows.astype(jnp.float32)
    normed = rms_norm(
        full_float, gain_mix_in, width, jnp.sum(full_float * full_float, axis=1, keepdims=True)
    ).astype(jnp.bfloat16)
    branch_cols = u_weight.shape[1]
    pieces = in_one_piece(
        (u_weight.astype(jnp.bfloat16), v_weight.astype(jnp.bfloat16)), "fs", 0, 1
    )
    u_pre = jnp.dot(normed, pieces[0], preferred_element_type=jnp.float32)
    v_pre = jnp.dot(normed, pieces[1], preferred_element_type=jnp.float32)
    u_act = jax.nn.gelu(u_pre * u_scale)
    v_act = jax.nn.gelu(v_pre * v_scale)
    total, squares = packed_total(
        (jnp.sum(v_act, axis=1, keepdims=True), jnp.sum(v_act * v_act, axis=1, keepdims=True)), "tp"
    )
    branch_width = branch_cols * lax.axis_size("tp")
    centre = total / branch_width
    spread = squares / branch_width - centre * centre
    v_norm = ((v_act - centre) * lax.rsqrt(spread + 1e-06) * v_gain).astype(jnp.bfloat16)
    groups = mix_matrix.shape[0]
    block = mix_matrix.shape[1]
    blocks = v_norm.reshape(rows // block, block, groups, branch_cols // groups)
    mixed = (
        jnp.einsum(
            "gts,bsgd->btgd",
            mix_matrix.astype(jnp.bfloat16),
            blocks,
            preferred_element_type=jnp.float32,
        )
        + mix_bias.T[None, :, :, None]
    )
    gated = (u_act * mixed.reshape(rows, branch_cols)).astype(jnp.bfloat16)
    partial_value = jnp.dot(
        gated,
        gathered_copies(out_weight.astype(jnp.bfloat16), "fs", 1),
        preferred_element_type=jnp.float32,
    )
    mix_out = (
        total_of_pieces(partial_value.astype(jnp.bfloat16), "tp").astype(jnp.float32) * out_scales
    )
    power = jnp.sum(mix_out * mix_out, axis=1, keepdims=True)
    middle_full = (full_float + rms_norm(mix_out, gain_mix_out, width, power)).astype(jnp.bfloat16)
    middle = lax.dynamic_slice_in_dim(middle_full, lane * part_width, part_width, 1)
    middle_float = middle_full.astype(jnp.float32)
    ffn_in = rms_norm(
        middle_float,
        gain_ffn_in,
        width,
        jnp.sum(middle_float * middle_float, axis=1, keepdims=True),
    ).astype(jnp.bfloat16)
    up_half = up_weight.astype(jnp.bfloat16)
    down_half = down_weight.astype(jnp.bfloat16)
    whole_up = lax.all_gather(up_half, "fs", axis=0, tiled=True)
    raised = jnp.dot(ffn_in, whole_up, preferred_element_type=jnp.float32)
    hidden = jnp.square(jax.nn.relu(raised * up_scale)).astype(jnp.bfloat16)
    whole_down = lax.all_gather(down_half, "fs", axis=1, tiled=True)
    terms = jnp.dot(hidden, whole_down, preferred_element_type=jnp.float32)
    own_down = lax.dynamic_slice_in_dim(down_scales, lane * part_width, part_width, 0)
    ffn_out = sent_and_summed(terms.astype(jnp.bfloat16), "tp", 1) * own_down
    power_out = over_copies(jnp.sum(ffn_out * ffn_out, axis=1, keepdims=True), "tp")
    own_gain_out = lax.dynamic_slice_in_dim(gain_ffn_out, lane * part_width, part_width, 0)
    return (middle.astype(jnp.float32) + rms_norm(ffn_out, own_gain_out, width, power_out)).astype(
        jnp.bfloat16
    )


def solution(mesh):
    in_specs = (
        P(("rep", "fs"), "tp"),
        P(),
        P("fs", "tp"),
        P("fs", "tp"),
        P("tp"),
        P("tp"),
        P("tp"),
        P("tp", None, None),
        P("tp", None),
        P("tp", "fs"),
        P("fs"),
        P(),
        P(),
        P("fs", "tp"),
        P("tp"),
        P("tp", "fs"),
        P("fs"),
        P(),
    )
    out_specs = P(("rep", "fs"), "tp")
    return jax.shard_map(local, mesh=mesh, in_specs=in_specs, out_specs=out_specs, check_vma=False)
```

profile of v0, /device:TPU:1, one launch (start us, length us, event | category | flops | bytes accessed | tf_op | source)
XLA Modules:
  0.0 657.6 jit_solution(17726470480720936505)
XLA Ops:
  6.5 0.7 all-gather.8.cloned.1.call-update
  7.3 0.0 all-gather.10.cloned.1.call-start
  7.3 0.9 convert_element_type.62
  8.2 0.9 convert_element_type.63
  9.1 0.7 pad_maximum_fusion
  9.8 0.0 all-gather.10.cloned.1.call-update
  9.8 0.9 convert_element_type.67
  10.8 18.3 %all-gather.8.cloned.1.call-done = bf16[1024,2048]{1,0:T(8,128)(2,1)} async-done(((bf16[1024,1024]{1,0:T(8,128)(2,1)}), bf16[1024,2048]{1,0:T(8,128)(2,1)}) %all-gather.8.cloned.1.call-update) | async-done | bytes 4194320 | tf_op jit(solution)/shard_map/all_gather | solution.py:103
  29.0 3.1 fusion.3
  32.1 135.9 %all-gather.10.cloned.1.call-done = bf16[2048,1024]{1,0:T(8,128)(2,1)} async-done(((bf16[64,1024]{1,0:T(8,128)(2,1)}), bf16[2048,1024]{1,0:T(8,128)(2,1)}) %all-gather.10.cloned.1.call-update) | async-done | bytes 4194320 | tf_op jit(solution)/shard_map/all_gather | solution.py:27
  168.0 5.8 fusion.68
  173.8 24.0 %all_to_all.21 = f32[2,1,2048]{2,1,0:T(1,128)S(1)} all-to-all(f32[2,1,2048]{2,1,0:T(1,128)S(1)} %broadcast_in_dim.6), channel_id=1, replica_groups=mesh['rep'=2,'fs'=32,'tp'=2] {'tp'}, dimensions={0} | all-to-all | bytes 32768 | tf_op jit(solution)/shard_map/all_to_all | solution.py:32
  197.8 1.6 broadcast_in_dim.7
  199.4 7.1 %all-to-all-start.1 = ((bf16[32,512,64]{1,2,0:T(8,128)(2,1)}), bf16[32,512,64]{1,2,0:T(8,128)(2,1)}, u32[]{:S(2)}, u32[]{:S(2)}) async-start(bf16[32,512,64]{1,2,0:T(8,128)(2,1)} %broadcast_in_dim.7), calls=%async_computation.1 | async-start | bytes 4194304 | tf_op jit(solution)/shard_map/all_to_all | solution.py:32
  206.5 0.0 all-gather.16.cloned.1.call-start
  206.6 0.3 multiply_convert_fusion.1
  206.9 2.1 reshape.90
  209.1 2.4 bitcast_add_fusion
  211.5 2.7 copy.55
  214.2 3.4 reshape.91
  217.6 15.7 %all-to-all-done.1 = bf16[32,512,64]{1,2,0:T(8,128)(2,1)} async-done(((bf16[32,512,64]{1,2,0:T(8,128)(2,1)}), bf16[32,512,64]{1,2,0:T(8,128)(2,1)}, u32[]{:S(2)}, u32[]{:S(2)}) %all-to-all-start.1) | async-done | bytes 2097184 | tf_op jit(solution)/shard_map/all_to_all | solution.py:32
  233.4 10.3 %convolution_convert_fusion = bf16[1024,2048]{1,0:T(8,128)(2,1)} fusion(bf16[512,2048]{0,1:T(8,128)(2,1)} %bitcast.5, f32[1024,512]{1,0:T(8,128)S(1)} %reshape.91, bf16[2048,1024]{1,0:T(8,128)(2,1)} %all-gather.10.cloned.1.call-done, bf16[1024,2048]{1,0:T(8,128)(2,1)} %all-gather.8.cloned.1.call-done, f32[2048]{0:T(1024)S(1)} %copy-done.10, ...), kind=kOutput, calls=%fused_computation.24 | convolution fusion | flops 4311220224 | bytes 14694400 | tf_op jit(solution)/shard_map/dot_general | solution.py:137
  243.7 0.0 all-gather.16.cloned.1.call-update
  243.8 0.0 all-gather.12.cloned.1.call-start
  243.8 1.0 copy-done.3
  244.8 0.7 convert_element_type.74
  245.5 0.0 all-gather.12.cloned.1.call-update
  245.5 0.0 all-gather.14.cloned.1.call-start
  245.6 0.7 convert_element_type.76
  246.3 0.0 all-gather.14.cloned.1.call-update
  246.4 66.4 %all-gather.1 = f32[32,64,2]{1,2,0:T(2,128)S(1)} all-gather(f32[1,64,2]{1,2,0:T(2,128)S(1)} %maximum_bitcast_fusion), channel_id=1, replica_groups=mesh['rep'=2,'fs'=32,'tp'=2] {'fs'}, dimensions={0}, use_global_device_ids=true | all-gather | bytes 16896 | tf_op jit(solution)/shard_map/all_gather | solution.py:11
  312.8 0.1 reshape.88
  312.9 0.0 all-gather.16.cloned.1.call-done
  313.0 9.9 %convert_reduce_fusion = f32[1024,2048]{1,0:T(8,128)} fusion(bf16[2,1024,2048]{2,1,0:T(8,128)(2,1)} %bitcast.34), kind=kLoop, calls=%fused_computation | loop fusion | flops 6291456 | bytes 16777216 | tf_op jit(solution)/shard_map/reduce_sum | solution.py:61
  322.9 4.5 multiply_reduce_fusion
  327.5 1.3 copy-done
  328.8 4.0 fusion
  332.8 82.2 %all-gather.12.cloned.1.call-done = bf16[2048,2048]{1,0:T(8,128)(2,1)} async-done(((bf16[64,2048]{1,0:T(8,128)(2,1)}), bf16[2048,2048]{1,0:T(8,128)(2,1)}) %all-gather.12.cloned.1.call-update) | async-done | bytes 8388624 | tf_op jit(solution)/shard_map/all_gather | solution.py:157
  415.0 167.9 %all-gather.14.cloned.1.call-done = bf16[2048,2048]{0,1:T(8,128)(2,1)} async-done(((bf16[2048,64]{0,1:T(8,128)(2,1)}), bf16[2048,2048]{0,1:T(8,128)(2,1)}) %all-gather.14.cloned.1.call-update) | async-done | bytes 8388624 | tf_op jit(solution)/shard_map/all_gather | solution.py:160
  582.9 25.7 %fusion.16 = bf16[1024,2048]{1,0:T(8,128)(2,1)} fusion(bf16[2048,2048]{0,1:T(8,128)(2,1)} %all-gather.14.cloned.1.call-done, bf16[2048,2048]{1,0:T(8,128)(2,1)} %all-gather.12.cloned.1.call-done, bf16[1024,2048]{1,0:T(8,128)(2,1)} %get-tuple-element.8, f32[2048]{0:T(1024)S(1)} %copy-done.11, f32[2048]{0:T(1024)S(1)} %copy-done.12, f32[1024]{0:T(1024)S(1)} %add_rsqrt_fusion.1), kind=kOutput, calls=%fused_computation.25 | convolution fusion | flops 17198743552 | bytes 25186304 | tf_op jit(solution)/shard_map/dot_general | solution.py:161
  608.5 2.6 copy.66
  611.2 27.7 %all_to_all.22 = bf16[2,1024,1024]{2,1,0:T(8,128)(2,1)S(1)} all-to-all(bf16[2,1024,1024]{2,1,0:T(8,128)(2,1)S(1)} %bitcast.33), channel_id=1, replica_groups=mesh['rep'=2,'fs'=32,'tp'=2] {'tp'}, dimensions={0} | all-to-all | bytes 8388608 | tf_op jit(solution)/shard_map/all_to_all | solution.py:71
  638.8 1.0 convert_reduce_fusion.1
  639.9 0.0 dynamic-slice-start
  639.9 1.9 copy-done.1
  641.8 0.5 multiply_reduce_fusion.1
  642.3 3.7 all_to_all.23
  646.1 5.0 add_convert_fusion
  (43 shorter events, 0.2 us)
Async XLA Ops:
  6.5 161.5 %copy-start.10 = (f32[2048]{0:T(1024)S(1)}, f32[2048]{0:T(1024)}, u32[]{:S(2)}) copy-start(f32[2048]{0:T(1024)} %param.19) | copy-start | bytes 24580
  6.5 161.5 %copy-start.13 = (f32[512]{0:T(512)S(1)}, f32[512]{0:T(512)}, u32[]{:S(2)}) copy-start(f32[512]{0:T(512)} %param.23) | copy-start | bytes 6148
  6.5 22.5 %all-gather.8.cloned.1.call-start = ((), (), s32[]{:S(2)}) async-start(), calls=%async_computation.4 | async-start | bytes 6291456 | tf_op jit(solution)/shard_map/all_gather | solution.py:103
  7.3 160.7 %all-gather.10.cloned.1.call-start = ((), (), s32[]{:S(2)}) async-start(), calls=%async_computation.5 | async-start | bytes 4325376 | tf_op jit(solution)/shard_map/all_gather | solution.py:27
  173.8 32.8 %copy-start.7 = (f32[512]{0:T(512)S(1)}, f32[512]{0:T(512)}, u32[]{:S(2)}) copy-start(f32[512]{0:T(512)} %param.24) | copy-start | bytes 6148
  199.4 34.0 %all-to-all-start.1 = ((bf16[32,512,64]{1,2,0:T(8,128)(2,1)}), bf16[32,512,64]{1,2,0:T(8,128)(2,1)}, u32[]{:S(2)}, u32[]{:S(2)}) async-start(bf16[32,512,64]{1,2,0:T(8,128)(2,1)} %broadcast_in_dim.7), calls=%async_computation.1 | async-start | bytes 4194304 | tf_op jit(solution)/shard_map/all_to_all | solution.py:32
  206.5 2.6 copy-start.6
  206.5 106.5 %all-gather.16.cloned.1.call-start = ((), (), s32[]{:S(2)}) async-start(), calls=%async_computation.8 | async-start | bytes 12582912 | tf_op jit(solution)/shard_map/all_gather | solution.py:60
  214.2 19.2 %copy-start.14 = (f32[512]{0:T(512)S(1)}, f32[512]{0:T(512)}, u32[]{:S(2)}) copy-start(f32[512]{0:T(512)} %param.22) | copy-start | bytes 6148
  243.7 1.0 copy-start.3
  243.7 1.9 copy-start.4
  243.7 2.6 copy-start.8
  243.7 2.6 copy-start.9
  243.8 171.2 %all-gather.12.cloned.1.call-start = ((), (), s32[]{:S(2)}) async-start(), calls=%async_computation.6 | async-start | bytes 8650752 | tf_op jit(solution)/shard_map/all_gather | solution.py:157
  245.5 337.3 %all-gather.14.cloned.1.call-start = ((), (), s32[]{:S(2)}) async-start(), calls=%async_computation.7 | async-start | bytes 8650752 | tf_op jit(solution)/shard_map/all_gather | solution.py:160
  313.0 14.5 %copy-start.2 = (bf16[1024,2048]{1,0:T(8,128)(2,1)S(1)}, bf16[1024,2048]{1,0:T(8,128)(2,1)}, u32[]{:S(2)}) copy-start(bf16[1024,2048]{1,0:T(8,128)(2,1)} %all-gather.8.cloned.1.call-done) | copy-start | bytes 12582916
  322.9 5.9 copy-start
  322.9 5.9 copy-start.5
  328.8 254.1 %copy-start.11 = (f32[2048]{0:T(1024)S(1)}, f32[2048]{0:T(1024)}, u32[]{:S(2)}) copy-start(f32[2048]{0:T(1024)} %param.32) | copy-start | bytes 24580
  328.8 254.1 %copy-start.12 = (f32[2048]{0:T(1024)S(1)}, f32[2048]{0:T(1024)}, u32[]{:S(2)}) copy-start(f32[2048]{0:T(1024)} %param.30) | copy-start | bytes 24580
  639.9 1.9 copy-start.1
  639.9 6.2 dynamic-slice-start
Sparse Core Ops, SparseCore 0:
  9.0 19.9 all-gather.7
  30.7 137.2 all-gather.9
  243.9 22.8 all-gather.15
  268.3 146.6 all-gather.11
  416.4 166.3 all-gather.13
where the time goes:
time: 658 us
  waiting for transfers between devices  421 us (64%)
  blocking collectives  122 us (19%)
  matrix products  44.2 us (7%)
  other arithmetic  33.3 us (5%)
  local copies, waits for them, and re-layouts  16.9 us (3%)
  between operations  13.4 us (2%)
  starting transfers between devices  7.24 us (1%)
    all_gather x1, waiting for transfers between devices, local(): whole_down = lax.all_gather(down_half, 'fs', axis=1, tiled=True)  168 us
    all_gather x1, waiting for transfers between devices, in_one_piece(): lax.all_gather(both, axis, axis=dim, tiled=True)  136 us
    all_gather x1, waiting for transfers between devices, local(): whole_up = lax.all_gather(up_half, 'fs', axis=0, tiled=True)  82.2 us
    all_gather x1, blocking collectives, turned_gather(): result = lax.all_gather(both, axis, axis=0, tiled=True)  66.4 us
    all_to_all x2, blocking collectives, copy_for_each(): return lax.all_to_all(copies, axis, split_axis=0, concat_axis=0, tiled=True)  27.7 us
    all_to_all x1, blocking collectives, sent_and_summed(): lax.all_to_all(in_blocks(array, dim, peers), axis, 0, 0, tiled=True)  27.7 us
    dot_general x1, matrix products, local(): terms = jnp.dot(hidden, whole_down, preferred_element_type=jnp.float32)  25.7 us
    all_gather x1, waiting for transfers between devices, local(): full_rows = lax.all_gather(resid, 'tp', axis=1, tiled=True)  18.3 us
  transfers between devices with their start and end apart: 6, of which 5 were waited for; matrix products, arithmetic and copies ran while one was open for 6% of the time, Pallas kernels for 0%

commit v1 on v0

--- a/solution.py
+++ b/solution.py
@@ -157,7 +157,9 @@
     whole_up = lax.all_gather(up_half, "fs", axis=0, tiled=True)
     raised = jnp.dot(ffn_in, whole_up, preferred_element_type=jnp.float32)
     hidden = jnp.square(jax.nn.relu(raised * up_scale)).astype(jnp.bfloat16)
-    whole_down = lax.all_gather(down_half, "fs", axis=1, tiled=True)
+    whole_down = jnp.concatenate(
+        lax.all_to_all(jnp.stack([down_half] * lax.axis_size("fs")), "fs", 0, 0), axis=1
+    )
     terms = jnp.dot(hidden, whole_down, preferred_element_type=jnp.float32)
     own_down = lax.dynamic_slice_in_dim(down_scales, lane * part_width, part_width, 0)
     ffn_out = sent_and_summed(terms.astype(jnp.bfloat16), "tp", 1) * own_down

time: 658 us -> 554 us (0.84)
  waiting for transfers between devices: 421 us -> 176 us
  blocking collectives: 122 us -> 252 us
    all_gather x1 -> x0, waiting for transfers between devices: 168 us -> none  [local(): whole_down = lax.all_gather(down_half, 'fs', axis=1, tiled=True)]
    all_gather x1, blocking collectives: 66.4 us -> 203 us  [turned_gather(): result = lax.all_gather(both, axis, axis=0, tiled=True)]
    all_gather x1, waiting for transfers between devices: 82.2 us -> 5.68 us  [local(): whole_up = lax.all_gather(up_half, 'fs', axis=0, tiled=True)]
  transfers between devices with their start and end apart: 6 -> 6, of which waited for: 5 -> 4; matrix products, arithmetic and copies ran while one was open for 6% -> 7% of each run, Pallas kernels for 0% -> 0%
where the time goes in v1:
time: 554 us; the launch traced here: 553 us
  blocking collectives  252 us (45%)
  waiting for transfers between devices  176 us (32%)
  matrix products  44.2 us (8%)
  other arithmetic  32.6 us (6%)
  local copies, waits for them, and re-layouts  21.2 us (4%)
  starting transfers between devices  13.4 us (2%)
  between operations  13.4 us (2%)
    all_gather x1, blocking collectives, turned_gather(): result = lax.all_gather(both, axis, axis=0, tiled=True)  203 us
    all_gather x1, waiting for transfers between devices, in_one_piece(): lax.all_gather(both, axis, axis=dim, tiled=True)  136 us
    all_to_all x2, blocking collectives, copy_for_each(): return lax.all_to_all(copies, axis, split_axis=0, concat_axis=0, tiled=True)  27.7 us
    dot_general x1, matrix products, local(): terms = jnp.dot(hidden, whole_down, preferred_element_type=jnp.float32)  25.6 us
    all_to_all x1, blocking collectives, sent_and_summed(): lax.all_to_all(in_blocks(array, dim, peers), axis, 0, 0, tiled=True)  21.8 us
    all_gather x1, waiting for transfers between devices, local(): full_rows = lax.all_gather(resid, 'tp', axis=1, tiled=True)  18.3 us
    all_to_all x1, waiting for transfers between devices, copy_for_each(): return lax.all_to_all(copies, axis, split_axis=0, concat_axis=0, tiled=True)  15.7 us
  transfers between devices with their start and end apart: 6, of which 4 were waited for; matrix products, arithmetic and copies ran while one was open for 7% of the time, Pallas kernels for 0%

profile of v1, /device:TPU:1, one launch (start us, length us, event | category | flops | bytes accessed | tf_op | source)
XLA Modules:
  0.0 553.4 jit_solution(16448828899005166675)
XLA Ops:
  6.5 0.7 all-gather.7.cloned.1.call-update
  7.3 0.0 all-gather.9.cloned.1.call-start
  7.3 0.9 convert_element_type.62
  8.2 0.9 convert_element_type.63
  9.1 0.7 pad_maximum_fusion
  9.8 0.0 all-gather.9.cloned.1.call-update
  9.8 0.9 convert_element_type.67
  10.8 18.3 %all-gather.7.cloned.1.call-done = bf16[1024,2048]{1,0:T(8,128)(2,1)} async-done(((bf16[1024,1024]{1,0:T(8,128)(2,1)}), bf16[1024,2048]{1,0:T(8,128)(2,1)}) %all-gather.7.cloned.1.call-update) | async-done | bytes 4194320 | tf_op jit(solution)/shard_map/all_gather | solution.py:103
  29.0 3.1 fusion.3
  32.1 135.9 %all-gather.9.cloned.1.call-done = bf16[2048,1024]{1,0:T(8,128)(2,1)} async-done(((bf16[64,1024]{1,0:T(8,128)(2,1)}), bf16[2048,1024]{1,0:T(8,128)(2,1)}) %all-gather.9.cloned.1.call-update) | async-done | bytes 4194320 | tf_op jit(solution)/shard_map/all_gather | solution.py:27
  168.0 5.8 %fusion.68 = (f32[1024]{0:T(1024)S(1)}, f32[1024]{0:T(1024)S(1)}, f32[1024,512]{1,0:T(8,128)S(1)}) fusion(f32[512]{0:T(512)S(1)} %copy-done.13, bf16[2048,1024]{1,0:T(8,128)(2,1)} %all-gather.9.cloned.1.call-done, bf16[1024,2048]{1,0:T(8,128)(2,1)} %all-gather.7.cloned.1.call-done, f32[2048]{0:T(1024)S(1)} %copy-done.10, f32[1024]{0:T(1024)S(1)} %add_rsqrt_fusion.3), kind=kOutput, calls=%fused_computation.78 | convolution fusion | flops 2162161664 | bytes 8411136 | tf_op jit(solution)/shard_map/dot_general | solution.py:114
  173.8 0.0 copy-start.7
  173.8 24.0 %all_to_all.26 = f32[2,1,2048]{2,1,0:T(1,128)S(1)} all-to-all(f32[2,1,2048]{2,1,0:T(1,128)S(1)} %broadcast_in_dim.6), channel_id=1, replica_groups=mesh['rep'=2,'fs'=32,'tp'=2] {'tp'}, dimensions={0} | all-to-all | bytes 32768 | tf_op jit(solution)/shard_map/all_to_all | solution.py:32
  197.8 1.6 broadcast_in_dim.7
  199.4 7.1 %all-to-all-start.1 = ((bf16[32,512,64]{1,2,0:T(8,128)(2,1)}), bf16[32,512,64]{1,2,0:T(8,128)(2,1)}, u32[]{:S(2)}, u32[]{:S(2)}) async-start(bf16[32,512,64]{1,2,0:T(8,128)(2,1)} %broadcast_in_dim.7), calls=%async_computation.1 | async-start | bytes 4194304 | tf_op jit(solution)/shard_map/all_to_all | solution.py:32
  206.5 0.0 copy-start.6
  206.5 0.0 all-gather.13.cloned.1.call-start
  206.6 0.3 multiply_convert_fusion.1
  206.9 2.1 reshape.100
  209.1 2.4 bitcast_add_fusion
  211.5 2.7 copy.56
  214.2 3.4 reshape.101
  217.6 15.7 %all-to-all-done.1 = bf16[32,512,64]{1,2,0:T(8,128)(2,1)} async-done(((bf16[32,512,64]{1,2,0:T(8,128)(2,1)}), bf16[32,512,64]{1,2,0:T(8,128)(2,1)}, u32[]{:S(2)}, u32[]{:S(2)}) %all-to-all-start.1) | async-done | bytes 2097184 | tf_op jit(solution)/shard_map/all_to_all | solution.py:32
  233.4 10.4 %convolution_convert_fusion = bf16[1024,2048]{1,0:T(8,128)(2,1)} fusion(bf16[512,2048]{0,1:T(8,128)(2,1)} %bitcast.5, f32[1024,512]{1,0:T(8,128)S(1)} %reshape.101, bf16[2048,1024]{1,0:T(8,128)(2,1)} %all-gather.9.cloned.1.call-done, bf16[1024,2048]{1,0:T(8,128)(2,1)} %all-gather.7.cloned.1.call-done, f32[2048]{0:T(1024)S(1)} %copy-done.10, ...), kind=kOutput, calls=%fused_computation.24 | convolution fusion | flops 4311220224 | bytes 14694400 | tf_op jit(solution)/shard_map/dot_general | solution.py:137
  243.8 0.0 all-gather.13.cloned.1.call-update
  243.8 0.0 all-gather.11.cloned.1.call-start
  243.9 1.0 copy-done.3
  244.9 0.7 convert_element_type.74
  245.6 0.0 all-gather.11.cloned.1.call-update
  245.7 4.3 stack.2
  250.0 6.2 %all-to-all-start.2 = ((bf16[32,2048,64]{1,2,0:T(8,128)(2,1)}), bf16[32,2048,64]{1,2,0:T(8,128)(2,1)}, u32[]{:S(2)}, u32[]{:S(2)}) async-start(bf16[32,2048,64]{1,2,0:T(8,128)(2,1)} %stack.2), calls=%async_computation.2 | async-start | bytes 16777216 | tf_op jit(solution)/shard_map/all_to_all | solution.py:161
  256.2 202.8 %all-gather.1 = f32[32,64,2]{1,2,0:T(2,128)S(1)} all-gather(f32[1,64,2]{1,2,0:T(2,128)S(1)} %maximum_bitcast_fusion), channel_id=1, replica_groups=mesh['rep'=2,'fs'=32,'tp'=2] {'fs'}, dimensions={0}, use_global_device_ids=true | all-gather | bytes 16896 | tf_op jit(solution)/shard_map/all_gather | solution.py:11
  459.0 0.1 reshape.98
  459.1 0.0 all-gather.13.cloned.1.call-done
  459.2 9.9 %convert_reduce_fusion = f32[1024,2048]{1,0:T(8,128)} fusion(bf16[2,1024,2048]{2,1,0:T(8,128)(2,1)} %bitcast.37), kind=kLoop, calls=%fused_computation | loop fusion | flops 6291456 | bytes 16777216 | tf_op jit(solution)/shard_map/reduce_sum | solution.py:61
  469.1 4.5 multiply_reduce_fusion
  473.6 1.3 copy-done
  474.9 4.0 fusion
  478.9 5.7 %all-gather.11.cloned.1.call-done = bf16[2048,2048]{1,0:T(8,128)(2,1)} async-done(((bf16[64,2048]{1,0:T(8,128)(2,1)}), bf16[2048,2048]{1,0:T(8,128)(2,1)}) %all-gather.11.cloned.1.call-update) | async-done | bytes 8388624 | tf_op jit(solution)/shard_map/all_gather | solution.py:157
  484.6 25.6 %fusion.16 = bf16[1024,2048]{1,0:T(8,128)(2,1)} fusion(bf16[2048,2048]{0,1:T(8,128)(2,1)} %bitcast.12, bf16[2048,2048]{1,0:T(8,128)(2,1)} %all-gather.11.cloned.1.call-done, bf16[1024,2048]{1,0:T(8,128)(2,1)} %get-tuple-element.8, f32[2048]{0:T(1024)S(1)} %copy-done.11, f32[2048]{0:T(1024)S(1)} %copy-done.12, f32[1024]{0:T(1024)S(1)} %add_rsqrt_fusion.1), kind=kOutput, calls=%fused_computation.25 | convolution fusion | flops 17198743552 | bytes 25186304 | tf_op jit(solution)/shard_map/dot_general | solution.py:163
  510.2 2.6 copy.67
  512.9 21.8 %all_to_all.27 = bf16[2,1024,1024]{2,1,0:T(8,128)(2,1)S(1)} all-to-all(bf16[2,1024,1024]{2,1,0:T(8,128)(2,1)S(1)} %bitcast.36), channel_id=1, replica_groups=mesh['rep'=2,'fs'=32,'tp'=2] {'tp'}, dimensions={0} | all-to-all | bytes 8388608 | tf_op jit(solution)/shard_map/all_to_all | solution.py:71
  534.6 1.0 convert_reduce_fusion.1
  535.7 0.0 dynamic-slice-start
  535.7 1.9 copy-done.1
  537.6 0.5 multiply_reduce_fusion.1
  538.1 3.7 all_to_all.28
  541.9 5.0 add_convert_fusion
  (43 shorter events, 0.2 us)
Async XLA Ops:
  6.5 161.5 %copy-start.10 = (f32[2048]{0:T(1024)S(1)}, f32[2048]{0:T(1024)}, u32[]{:S(2)}) copy-start(f32[2048]{0:T(1024)} %param.19) | copy-start | bytes 24580
  6.5 161.5 %copy-start.13 = (f32[512]{0:T(512)S(1)}, f32[512]{0:T(512)}, u32[]{:S(2)}) copy-start(f32[512]{0:T(512)} %param.23) | copy-start | bytes 6148
  6.5 22.5 %all-gather.7.cloned.1.call-start = ((), (), s32[]{:S(2)}) async-start(), calls=%async_computation.5 | async-start | bytes 6291456 | tf_op jit(solution)/shard_map/all_gather | solution.py:103
  7.3 160.7 %all-gather.9.cloned.1.call-start = ((), (), s32[]{:S(2)}) async-start(), calls=%async_computation.6 | async-start | bytes 4325376 | tf_op jit(solution)/shard_map/all_gather | solution.py:27
  173.8 32.8 %copy-start.7 = (f32[512]{0:T(512)S(1)}, f32[512]{0:T(512)}, u32[]{:S(2)}) copy-start(f32[512]{0:T(512)} %param.24) | copy-start | bytes 6148
  199.4 34.0 %all-to-all-start.1 = ((bf16[32,512,64]{1,2,0:T(8,128)(2,1)}), bf16[32,512,64]{1,2,0:T(8,128)(2,1)}, u32[]{:S(2)}, u32[]{:S(2)}) async-start(bf16[32,512,64]{1,2,0:T(8,128)(2,1)} %broadcast_in_dim.7), calls=%async_computation.1 | async-start | bytes 4194304 | tf_op jit(solution)/shard_map/all_to_all | solution.py:32
  206.5 2.6 copy-start.6
  206.5 252.7 %all-gather.13.cloned.1.call-start = ((), (), s32[]{:S(2)}) async-start(), calls=%async_computation.8 | async-start | bytes 12582912 | tf_op jit(solution)/shard_map/all_gather | solution.py:60
  214.2 19.2 %copy-start.14 = (f32[512]{0:T(512)S(1)}, f32[512]{0:T(512)}, u32[]{:S(2)}) copy-start(f32[512]{0:T(512)} %param.22) | copy-start | bytes 6148
  243.8 1.0 copy-start.3
  243.8 1.8 copy-start.4
  243.8 240.8 %all-gather.11.cloned.1.call-start = ((), (), s32[]{:S(2)}) async-start(), calls=%async_computation.7 | async-start | bytes 8650752 | tf_op jit(solution)/shard_map/all_gather | solution.py:157
  250.0 6.2 %copy-start.8 = (f32[64]{0:T(128)S(1)}, f32[64]{0:T(128)}, u32[]{:S(2)}) copy-start(f32[64]{0:T(128)} %param.34) | copy-start | bytes 772
  250.0 6.2 %copy-start.9 = (f32[64]{0:T(128)S(1)}, f32[64]{0:T(128)}, u32[]{:S(2)}) copy-start(f32[64]{0:T(128)} %param.28) | copy-start | bytes 772
  250.0 229.0 %all-to-all-start.2 = ((bf16[32,2048,64]{1,2,0:T(8,128)(2,1)}), bf16[32,2048,64]{1,2,0:T(8,128)(2,1)}, u32[]{:S(2)}, u32[]{:S(2)}) async-start(bf16[32,2048,64]{1,2,0:T(8,128)(2,1)} %stack.2), calls=%async_computation.2 | async-start | bytes 16777216 | tf_op jit(solution)/shard_map/all_to_all | solution.py:161
  459.2 14.4 %copy-start.2 = (bf16[1024,2048]{1,0:T(8,128)(2,1)S(1)}, bf16[1024,2048]{1,0:T(8,128)(2,1)}, u32[]{:S(2)}) copy-start(bf16[1024,2048]{1,0:T(8,128)(2,1)} %all-gather.7.cloned.1.call-done) | copy-start | bytes 12582916
  469.1 5.9 %copy-start = (f32[1024,2048]{1,0:T(8,128)S(1)}, f32[1024,2048]{1,0:T(8,128)}, u32[]{:S(2)}) copy-start(f32[1024,2048]{1,0:T(8,128)} %convert_reduce_fusion) | copy-start | bytes 25165828
  469.1 5.9 %copy-start.5 = (f32[2048]{0:T(1024)S(1)}, f32[2048]{0:T(1024)}, u32[]{:S(2)}) copy-start(f32[2048]{0:T(1024)} %param.29) | copy-start | bytes 24580
  474.9 9.7 %copy-start.11 = (f32[2048]{0:T(1024)S(1)}, f32[2048]{0:T(1024)}, u32[]{:S(2)}) copy-start(f32[2048]{0:T(1024)} %param.32) | copy-start | bytes 24580
  474.9 9.7 %copy-start.12 = (f32[2048]{0:T(1024)S(1)}, f32[2048]{0:T(1024)}, u32[]{:S(2)}) copy-start(f32[2048]{0:T(1024)} %param.30) | copy-start | bytes 24580
  535.7 1.9 copy-start.1
  535.7 6.2 %dynamic-slice-start = ((f32[2048]{0:T(1024)}, s32[]{:T(128)}), f32[1024]{0:T(1024)S(1)}, s32[]{:S(2)}) async-start(f32[2048]{0:T(1024)} %param.35, s32[]{:T(128)} %select_n.2), calls=%async_computation.9 | async-start | bytes 8704 | tf_op jit(solution)/shard_map/dynamic_slice | solution.py:167
Sparse Core Ops, SparseCore 0:
  9.0 19.9 all-gather.6
  30.7 137.2 all-gather.8
  244.0 22.8 all-gather.12
  268.3 216.2 all-gather.10
